TPU v7x, 32 devices: a whole 2x2x4 slice. The times are simulated.
32 devices in a mesh: ep: 8 (over z, y), tp: 4 (over x, core).
Axes of the slice: x: 2, y: 2, z: 4, core: 2. Of those that a mesh axis runs over, the one named last changes fastest.
Arguments:
- tokens: bfloat16 [128, 1024], P('ep'), may hold values from -24 to 24
- seq_length: int32 [128], P('ep'), may hold values from 1024 to 16383
- ret_state: float32 [128, 4, 128, 256], P('ep', 'tp'), may hold values from -0.6 to 0.6
- norm_in: float32 [1024], replicated, may hold values from 0.1 to 1.9
- w_query: bfloat16 [1024, 512], P(None, 'tp'), may hold values from -0.1875 to 0.1875
- w_key: bfloat16 [1024, 512], P(None, 'tp'), may hold values from -0.1875 to 0.1875
- w_value: bfloat16 [1024, 1024], P(None, 'tp'), may hold values from -0.1875 to 0.1875
- head_gain: float32 [1024], P('tp'), may hold values from 0.1 to 1.9
- w_output: bfloat16 [1024, 1024], P('tp'), may hold values from -0.1875 to 0.1875
- norm_mid: float32 [1024], replicated, may hold values from 0.1 to 1.9
- route_expert: int32 [128, 2], P('ep'), may hold values from 0 to 3, all different within a row; in each aligned block of 16 rows (0 to 15, 16 to 31, ...) at most 12 rows name the same one
- route_score: float32 [128, 2], P('ep'), may hold values from -6 to 6
- expert_gate: bfloat16 [8, 1024, 1792], P('ep', None, 'tp'), may hold values from -0.1875 to 0.1875
- expert_up: bfloat16 [8, 1024, 1792], P('ep', None, 'tp'), may hold values from -0.1875 to 0.1875
- expert_down: bfloat16 [8, 1792, 1024], P('ep', 'tp'), may hold values from -0.09375 to 0.09375
Outputs:
- mixed: bfloat16 [128, 1024], P('ep', 'tp')
Inputs may be any that keep to these rules, and one draw needn't show every extreme that they name: `route_expert`: each row names 2 different experts; within the rows of one device no expert is named by more than 12 rows, and some device's rows name one expert exactly 12 times.
All inputs are finite; a program needn't handle non-finite values.
Results may differ from a plain program's by a relative error of at most 0.014.
Values may be sent and summed in bfloat16 or wider, within the bound.
A program may use at most 64 MiB of HBM per device.

v0:
```python
import jax
import jax.numpy as jnp
from jax import lax
from jax.sharding import PartitionSpec as P

DK = 128
DV = 256
SPREAD = 2
TOP_K = 2


EPS = 1e-06


def rotate(head_rows, positions):
    half_width = head_rows.shape[-1] // 2
    inverse = 10000.0 ** (-jnp.arange(half_width, dtype=jnp.float32) / half_width)
    angles = positions[:, None] * inverse[None, :]
    cosine = jnp.cos(angles)[:, None, :]
    sine_part = jnp.sin(angles)[:, None, :]
    first_half = head_rows[..., :half_width]
    second = head_rows[..., half_width:]
    return jnp.concatenate(
        [first_half * cosine - second * sine_part, first_half * sine_part + second * cosine],
        axis=-1,
    )


def body(
    tokens,
    seq_length,
    ret_state,
    norm_in,
    w_query,
    w_key,
    w_value,
    head_gain,
    w_output,
    norm_mid,
    route_expert,
    route_score,
    expert_gate,
    expert_up,
    expert_down,
):
    n_lanes = lax.axis_size("tp")
    n_groups = lax.axis_size("ep")
    lane_index = lax.axis_index("tp")
    local_rows = tokens.shape[0]
    width = tokens.shape[1]
    quarter = width // n_lanes
    heads_here = w_query.shape[1] // DK
    token_f = tokens.astype(jnp.float32)
    normed = (
        token_f * lax.rsqrt(jnp.mean(token_f * token_f, axis=-1, keepdims=True) + EPS) * norm_in
    ).astype(jnp.bfloat16)
    query_proj = jnp.dot(normed, w_query, preferred_element_type=jnp.float32).astype(jnp.bfloat16)
    key_proj = jnp.dot(normed, w_key, preferred_element_type=jnp.float32).astype(jnp.bfloat16)
    value_proj = jnp.dot(normed, w_value, preferred_element_type=jnp.float32).astype(jnp.bfloat16)
    positions = seq_length.astype(jnp.float32)
    q_rot = rotate(query_proj.astype(jnp.float32).reshape(local_rows, heads_here, DK), positions)
    k_rot = rotate(
        key_proj.astype(jnp.float32).reshape(local_rows, heads_here, DK), positions
    ) * DK ** (-0.5)
    value_rows = value_proj.astype(jnp.float32).reshape(local_rows, heads_here, DV)
    head_index = (lane_index * heads_here + jnp.arange(heads_here, dtype=jnp.int32)).astype(
        jnp.float32
    )
    decay_rate = 1.0 - jnp.exp2(-2.0 - 2.0 * head_index)
    carried = jnp.einsum("bhd,bhde->bhe", q_rot, ret_state, precision=lax.Precision.HIGHEST)
    within = jnp.sum(q_rot * k_rot, axis=-1, keepdims=True) * value_rows
    retained = decay_rate[None, :, None] * carried + within
    centre = jnp.mean(retained, axis=-1, keepdims=True)
    variance = jnp.mean(jnp.square(retained - centre), axis=-1, keepdims=True)
    ret_out = ((retained - centre) * lax.rsqrt(variance + EPS)).reshape(local_rows, heads_here * DV)
    ret_out = (ret_out * head_gain).astype(jnp.bfloat16)
    partial_value = jnp.dot(ret_out, w_output, preferred_element_type=jnp.float32)
    experts_n = n_groups // SPREAD
    cap = min(local_rows, max(2, 3 * local_rows * TOP_K // (2 * experts_n)))
    flat_rows = route_expert.reshape(-1)
    onehot = (flat_rows[:, None] == jnp.arange(experts_n, dtype=jnp.int32)[None, :]).astype(
        jnp.int32
    )
    rank_index = jnp.sum((jnp.cumsum(onehot, axis=0) - onehot) * onehot, axis=1)
    slot_index = flat_rows * cap + rank_index
    chosen_slot = (
        slot_index[:, None] == jnp.arange(experts_n * cap, dtype=jnp.int32)[None, :]
    ).astype(jnp.float32)
    chosen_slot = chosen_slot.reshape(local_rows, TOP_K, experts_n * cap)
    placing = jnp.sum(chosen_slot, axis=1).astype(jnp.bfloat16)
    weights = jax.nn.softmax(route_score, axis=-1)
    combine = jnp.sum(chosen_slot * weights[:, :, None], axis=1)
    gate_rows = expert_gate[0]
    up_rows = expert_up[0]
    down_rows = expert_down[0]
    attended = lax.psum(partial_value.astype(jnp.bfloat16), "tp").astype(jnp.float32)
    resid_full = (token_f + attended).astype(jnp.bfloat16)
    resid_f = resid_full.astype(jnp.float32)
    mid_full = (
        resid_f * lax.rsqrt(jnp.mean(resid_f * resid_f, axis=-1, keepdims=True) + EPS) * norm_mid
    ).astype(jnp.bfloat16)
    resid = lax.dynamic_slice_in_dim(resid_full, lane_index * quarter, quarter, 1)
    mid = lax.dynamic_slice_in_dim(mid_full, lane_index * quarter, quarter, 1)
    packed = jnp.einsum("re,rc->ec", placing, mid, preferred_element_type=jnp.float32).astype(
        jnp.bfloat16
    )
    packed = packed.reshape(experts_n, cap, quarter)
    send_buffer = jnp.repeat(packed, SPREAD, axis=0)
    received = lax.all_to_all(send_buffer, "ep", split_axis=0, concat_axis=0, tiled=True)
    groups, row_count, cols = received.shape
    piece_cols = lax.all_gather(received, "tp", axis=2, tiled=True)
    piece_width = piece_cols.shape[2]
    flat_in = piece_cols.reshape(groups * row_count, piece_width)
    gate_sum = jnp.dot(flat_in, gate_rows, preferred_element_type=jnp.float32)
    up_sum = jnp.dot(flat_in, up_rows, preferred_element_type=jnp.float32)
    hidden = (jax.nn.silu(gate_sum) * up_sum).astype(jnp.bfloat16)
    down_part = jnp.dot(hidden, down_rows, preferred_element_type=jnp.float32)
    share = lax.psum_scatter(
        down_part.astype(jnp.bfloat16), "tp", scatter_dimension=1, tiled=True
    ).astype(jnp.float32)
    returned = share.astype(jnp.bfloat16).reshape(groups, row_count, share.shape[1])
    arrived = lax.all_to_all(returned, "ep", split_axis=0, concat_axis=0, tiled=True)
    part_total = jnp.sum(
        arrived.reshape(experts_n, SPREAD, cap, quarter).astype(jnp.float32), axis=1
    )
    expert_out = part_total.astype(jnp.bfloat16)
    expert_mix = jnp.dot(
        combine,
        expert_out.reshape(experts_n * cap, quarter).astype(jnp.float32),
        precision=lax.Precision.HIGHEST,
    )
    return (resid.astype(jnp.float32) + expert_mix).astype(jnp.bfloat16)


def solution(mesh):
    placed = (
        P("ep", None),
        P("ep"),
        P("ep", "tp", None, None),
        P(),
        P(None, "tp"),
        P(None, "tp"),
        P(None, "tp"),
        P("tp"),
        P("tp", None),
        P(),
        P("ep", None),
        P("ep", None),
        P("ep", None, "tp"),
        P("ep", None, "tp"),
        P("ep", "tp", None),
    )
    return jax.shard_map(body, mesh=mesh, in_specs=placed, out_specs=P("ep", "tp"), check_vma=False)
```

profile of v0, /device:TPU:0, one launch (start us, length us, event | category | flops | bytes accessed | tf_op | source)
XLA Modules:
  0.0 89.4 jit_solution(11786482664120521328)
XLA Ops:
  6.5 0.0 copy-start
  6.5 0.0 copy-start.3
  6.5 0.0 copy-start.7
  6.5 0.0 copy-start.5
  6.5 0.0 reduce-scatter.2.cloned.1.call-start
  6.7 0.8 reduce_max.9
  7.5 0.7 fusion.51
  8.2 0.7 fusion.50
  8.9 0.7 convert_element_type.79
  9.5 0.9 fusion.22
  10.4 0.0 copy-start.4
  10.4 1.2 %fusion.10 = f32[16,1,128]{2,0,1:T(8,128)S(1)} fusion(bf16[1024,128]{1,0:T(8,128)(2,1)} %param.20, bf16[16,1024]{1,0:T(8,128)(2,1)} %param.15, f32[1024]{0:T(1024)} %param.18, f32[16]{0:T(128)S(1)} %add_rsqrt_fusion.2), kind=kOutput, calls=%fused_computation.18 | convolution fusion | flops 4263936 | bytes 307264 | tf_op jit(solution)/shard_map/dot_general | solution.py:58
  11.6 1.2 %fusion.8 = f32[16,1,128]{2,0,1:T(8,128)S(1)} fusion(bf16[1024,128]{1,0:T(8,128)(2,1)} %param.19, bf16[16,1024]{1,0:T(8,128)(2,1)} %param.15, f32[1024]{0:T(1024)} %param.18, f32[16]{0:T(128)S(1)} %add_rsqrt_fusion.2), kind=kOutput, calls=%fused_computation.16 | convolution fusion | flops 4263936 | bytes 307264 | tf_op jit(solution)/shard_map/dot_general | solution.py:57
  12.8 0.8 copy.28
  13.6 0.1 eq.29
  13.7 0.0 copy-start.6
  13.7 0.0 copy-start.2
  13.7 0.1 fusion.37
  13.8 0.2 fusion.45
  14.0 0.0 copy-done
  14.0 0.0 copy-start.1
  14.0 1.1 %fusion = f32[16,1,256]{2,1,0:T(1,128)S(1)} fusion(f32[16,128,1]{1,2,0:T(1,128)S(1)} %bitcast.45, f32[16,1,128,256]{3,2,1,0:T(8,128)S(1)} %copy-done), kind=kOutput, calls=%fused_computation | convolution fusion | flops 6291456 | bytes 2121728 | tf_op jit(solution)/shard_map/bhd,bhde->bhe/dot_general | solution.py:70
  15.1 0.0 copy-done.3
  15.1 0.0 copy-done.7
  15.1 0.0 copy-done.6
  15.2 0.3 fusion.58
  15.5 0.2 multiply_reduce_fusion.1
  15.7 0.0 copy-done.5
  15.7 0.0 copy-done.2
  15.7 0.2 convolution_convert_fusion.1
  15.9 12.9 %psum.7 = bf16[16,1024]{1,0:T(8,128)(2,1)S(1)} all-reduce(bf16[16,1024]{1,0:T(8,128)(2,1)S(1)} %convolution_convert_fusion.1), channel_id=1, replica_groups=mesh['ep'=8,'tp'=4] {'tp'}, use_global_device_ids=true, to_apply=%region_4.0 | all-reduce | flops 16384 | bytes 65536 | tf_op jit(solution)/shard_map/psum | solution.py:96
  28.8 0.1 multiply_reduce_fusion
  29.0 0.1 fusion.28
  29.0 0.1 reduce_window_sum.11
  29.1 0.2 select_reduce_fusion.1
  29.3 0.1 reduce_sum.100
  29.4 0.1 copy.29
  29.5 0.0 copy-done.4
  29.5 0.8 dynamic-slice
  30.3 0.1 convert_reduce_fusion
  30.3 0.2 convolution_convert_fusion.2
  30.6 12.5 %all_to_all.10 = bf16[8,12,256]{2,1,0:T(8,128)(2,1)S(1)} all-to-all(bf16[8,12,256]{2,1,0:T(8,128)(2,1)S(1)} %bitcast.44), channel_id=1, replica_groups=mesh['ep'=8,'tp'=4] {'ep'}, dimensions={0} | all-to-all | bytes 98304 | tf_op jit(solution)/shard_map/all_to_all | solution.py:109
  43.1 5.8 %all_gather.3 = bf16[8,12,1024]{2,1,0:T(8,128)(2,1)S(1)} all-gather(bf16[8,12,256]{2,1,0:T(8,128)(2,1)S(1)} %all_to_all.10), channel_id=1, replica_groups=mesh['ep'=8,'tp'=4] {'tp'}, dimensions={2}, use_global_device_ids=true | all-gather | bytes 245760 | tf_op jit(solution)/shard_map/all_gather | solution.py:111
  48.9 0.0 copy-done.1
  48.9 0.4 fusion.14
  49.4 2.8 %convolution_convert_fusion = bf16[96,1024]{1,0:T(8,128)(2,1)} fusion(bf16[96,1024]{1,0:T(8,128)(2,1)S(1)} %reshape.273, bf16[1,448,1024]{2,1,0:T(8,128)(2,1)} %param.29, bf16[1,1024,448]{1,2,0:T(8,128)(2,1)} %param.28, f32[96,448]{1,0:T(8,128)S(1)} %fusion.14), kind=kOutput, calls=%fused_computation.2 | convolution fusion | flops 176517120 | bytes 2400256 | tf_op jit(solution)/shard_map/dot_general | solution.py:117
  52.2 0.0 reduce-scatter.2.cloned.1.call-update
  52.2 16.5 %reduce-scatter.2.cloned.1.call-done = bf16[96,256]{1,0:T(8,128)(2,1)} async-done(((bf16[96,1024]{1,0:T(8,128)(2,1)}), bf16[96,256]{1,0:T(8,128)(2,1)}) %reduce-scatter.2.cloned.1.call-update) | async-done | bytes 49168 | tf_op jit(solution)/shard_map/reduce_scatter | solution.py:118
  68.7 0.8 reshape.274
  69.5 12.2 %all_to_all.11 = bf16[8,12,256]{2,1,0:T(8,128)(2,1)S(1)} all-to-all(bf16[8,12,256]{2,1,0:T(8,128)(2,1)S(1)} %reshape.274), channel_id=1, replica_groups=mesh['ep'=8,'tp'=4] {'ep'}, dimensions={0} | all-to-all | bytes 98304 | tf_op jit(solution)/shard_map/all_to_all | solution.py:122
  81.8 0.7 fusion.3
  (12 shorter events, 0.2 us)
Async XLA Ops:
  6.5 7.5 %copy-start = (f32[16,1,128,256]{3,2,1,0:T(8,128)S(1)}, f32[16,1,128,256]{3,2,1,0:T(8,128)}, u32[]{:S(2)}) copy-start(f32[16,1,128,256]{3,2,1,0:T(8,128)} %param.17) | copy-start | bytes 6291460
  6.5 8.6 %copy-start.3 = (bf16[16,1024]{1,0:T(8,128)(2,1)S(1)}, bf16[16,1024]{1,0:T(8,128)(2,1)}, u32[]{:S(2)}) copy-start(bf16[16,1024]{1,0:T(8,128)(2,1)} %param.15) | copy-start | bytes 98308
  6.5 8.6 %copy-start.7 = (f32[1024]{0:T(1024)S(1)}, f32[1024]{0:T(1024)}, u32[]{:S(2)}) copy-start(f32[1024]{0:T(1024)} %param.18) | copy-start | bytes 12292
  6.5 9.2 %copy-start.5 = (f32[256]{0:T(256)S(1)}, f32[256]{0:T(256)}, u32[]{:S(2)}) copy-start(f32[256]{0:T(256)} %param.22) | copy-start | bytes 3076
  6.5 62.2 %reduce-scatter.2.cloned.1.call-start = ((), (), s32[]{:S(2)}) async-start(), calls=%async_computation.3 | async-start | bytes 245760 | tf_op jit(solution)/shard_map/reduce_scatter | solution.py:118
  10.4 19.1 %copy-start.4 = (s32[16,2]{0,1:T(2,128)S(1)}, s32[16,2]{0,1:T(2,128)}, u32[]{:S(2)}) copy-start(s32[16,2]{0,1:T(2,128)} %param.25) | copy-start | bytes 388
  13.7 1.5 %copy-start.6 = (bf16[1024,256]{1,0:T(8,128)(2,1)S(1)}, bf16[1024,256]{1,0:T(8,128)(2,1)}, u32[]{:S(2)}) copy-start(bf16[1024,256]{1,0:T(8,128)(2,1)} %param.21) | copy-start | bytes 1572868
  13.7 2.0 %copy-start.2 = (bf16[256,1024]{1,0:T(8,128)(2,1)S(1)}, bf16[256,1024]{1,0:T(8,128)(2,1)}, u32[]{:S(2)}) copy-start(bf16[256,1024]{1,0:T(8,128)(2,1)} %param.23) | copy-start | bytes 1572868
  14.0 34.9 %copy-start.1 = (bf16[1,1024,448]{1,2,0:T(8,128)(2,1)S(1)}, bf16[1,1024,448]{1,2,0:T(8,128)(2,1)}, u32[]{:S(2)}) copy-start(bf16[1,1024,448]{1,2,0:T(8,128)(2,1)} %param.27) | copy-start | bytes 2752516
Sparse Core Ops, SparseCore 0:
  52.3 16.3 reduce-scatter.1
where the time goes:
time: 89.9 us; the launch traced here: 89.4 us
  blocking collectives  43.4 us (48%)
  waiting for transfers between devices  16.5 us (18%)
  between operations  13.6 us (15%)
  matrix products  8.21 us (9%)
  other arithmetic  4.82 us (5%)
  local copies, waits for them, and re-layouts  2.74 us (3%)
    reduce_scatter x1, waiting for transfers between devices, body(): lax.psum_scatter(down_part.astype(jnp.bfloat16), 'tp', scatter_dimension=...  16.5 us
    psum x1, blocking collectives, body(): lax.psum(partial_value.astype(jnp.bfloat16), 'tp').astype(jnp.float32)  12.9 us
    all_to_all x1, blocking collectives, body(): lax.all_to_all(send_buffer, 'ep', split_axis=0, concat_axis=0, tiled=True)  12.5 us
    all_to_all x1, blocking collectives, body(): lax.all_to_all(returned, 'ep', split_axis=0, concat_axis=0, tiled=True)  12.2 us
    all_gather x1, blocking collectives, body(): piece_cols = lax.all_gather(received, 'tp', axis=2, tiled=True)  5.76 us
    dot_general x1, matrix products, body(): down_part = jnp.dot(hidden, down_rows, preferred_element_type=jnp.float32)  2.82 us
  transfers between devices with their start and end apart: 1, of which 1 were waited for; matrix products, arithmetic and copies ran while one was open for 0% of the time, Pallas kernels for 0%

commit v1 on v0

v1 whole, which is shorter than its diff:
```python
import functools

import jax
import jax.numpy as jnp
import numpy as np
from jax import lax
from jax.experimental import pallas as pl
from jax.experimental.pallas import tpu as pltpu
from jax.sharding import PartitionSpec as P

DK = 128
DV = 256
SPREAD = 2
CORES = 2
EPS = 1e-06
F32 = jnp.float32
BF16 = jnp.bfloat16


def each(low, high, step):
    if high - low <= 8:
        for index in range(low, high):
            step(index)
    else:

        def one(index, carry):
            step(index)
            return carry

        lax.fori_loop(low, high, one, 0)


def dot_rows(left, right):
    return lax.dot_general(left, right, (((1,), (1,)), ((), ())), preferred_element_type=F32)


def sin_cos(angles):
    turns = jnp.floor(angles * np.float32(2.0 / np.pi) + 0.5)
    rest = angles - turns * np.float32(1.5703125)
    rest = rest - turns * np.float32(4.837512969970703125e-4)
    rest = rest - turns * np.float32(7.54978995489188216e-8)
    square = rest * rest
    sine = rest + rest * square * (
        -1.6666654611e-1 + square * (8.3321608736e-3 - square * 1.9515295891e-4)
    )
    cosine = 1.0 - 0.5 * square + square * square * (
        4.166664568298827e-2 + square * (-1.388731625493765e-3 + square * 2.443315711809948e-5)
    )
    quarter = turns - 4.0 * jnp.floor(turns * 0.25)
    odd = (quarter == 1.0) | (quarter == 3.0)
    sin_base = jnp.where(odd, cosine, sine)
    cos_base = jnp.where(odd, sine, cosine)
    sin_value = jnp.where(quarter >= 2.0, -sin_base, sin_base)
    cos_value = jnp.where((quarter == 1.0) | (quarter == 2.0), -cos_base, cos_base)
    return sin_value, cos_value


def kernel(
    n_ep,
    n_tp,
    tokens,
    seq_length,
    inverse,
    norm_in,
    head_gain,
    norm_mid,
    route_expert,
    route_score,
    state_hbm,
    wq_hbm,
    wk_hbm,
    wv_hbm,
    wo_hbm,
    gate_hbm,
    up_hbm,
    down_hbm,
    out,
    state,
    wq,
    wk,
    wv,
    wo,
    gate,
    up,
    down,
    carried,
    part,
    part_in,
    resid,
    rows,
    hidden,
    pair_out,
    pair_in,
    own_sum,
    share,
    arrived,
    load_sem,
    tp_send,
    tp_recv,
    row_send,
    row_recv,
    fwd_send,
    fwd_recv,
    pair_send,
    pair_recv,
    ret_send,
    ret_recv,
):
    n_x = n_tp // CORES
    e = lax.axis_index("ep")
    t = lax.axis_index("tp")
    x = t // CORES
    c = t % CORES
    sibling = x * CORES + 1 - c
    n_rows = tokens.shape[0]
    width = tokens.shape[1]
    half = width // CORES
    quarter = width // n_tp
    heads = wq.shape[1] // DK
    n_state = 4 if n_rows % 4 == 0 else 1
    per = n_rows // n_state

    def to(ep_index, tp_index):
        return (ep_index, tp_index)

    barrier = pltpu.get_barrier_semaphore()

    def greet(d):
        for dx in range(n_x):
            peer = to((e + d) % n_ep, ((x + dx) % n_x) * CORES + c)
            pl.semaphore_signal(
                barrier, inc=1, device_id=peer, device_id_type=pl.DeviceIdType.MESH
            )

    loads = []
    pairs = [(wq_hbm, wq), (wk_hbm, wk), (wv_hbm, wv)]
    for i in range(n_state):
        pairs.append((state_hbm.at[pl.ds(i * per, per)], state.at[pl.ds(i * per, per)]))
    pairs += [
        (wo_hbm, wo),
        (gate_hbm.at[0], gate),
        (up_hbm.at[0], up),
        (down_hbm.at[0], down),
    ]
    for i, (source, target) in enumerate(pairs):
        load = pltpu.make_async_copy(source, target, load_sem.at[i])
        load.start()
        loads.append(load)
    for dx in range(1, n_x):
        peer = to(e, ((x + dx) % n_x) * CORES + c)
        pl.semaphore_signal(barrier, inc=1, device_id=peer, device_id_type=pl.DeviceIdType.MESH)
    for dx in range(n_x):
        peer = to(e, ((x + dx) % n_x) * CORES + 1 - c)
        pl.semaphore_signal(barrier, inc=1, device_id=peer, device_id_type=pl.DeviceIdType.MESH)
    each(1, n_ep, greet)

    token_f = tokens[...].astype(F32)
    scale = lax.rsqrt(jnp.mean(token_f * token_f, axis=-1, keepdims=True) + EPS)
    normed = (token_f * scale * norm_in[...]).astype(BF16)
    eye = lax.broadcasted_iota(jnp.int32, (n_rows, n_rows), 0) == lax.broadcasted_iota(
        jnp.int32, (n_rows, n_rows), 1
    )

    def column(row):
        return jnp.sum(jnp.where(eye, row, 0.0), axis=-1, keepdims=True)

    positions = column(seq_length[...].astype(F32))
    sine, cosine = sin_cos(positions * inverse[...])
    low_half = lax.broadcasted_iota(jnp.int32, (n_rows, DK), 1) < DK // 2
    sine = jnp.where(low_half, -sine, sine)
    score = route_score[...]
    raised = jnp.exp(score - jnp.max(score, axis=0, keepdims=True))
    softmax = raised / jnp.sum(raised, axis=0, keepdims=True)

    top_k = route_expert.shape[0]
    chosen = [column(route_expert[j : j + 1, :].astype(F32)) for j in range(top_k)]
    weights = [column(softmax[j : j + 1, :]) for j in range(top_k)]

    loads[0].wait()
    query = jnp.dot(normed, wq[...], preferred_element_type=F32).astype(BF16).astype(F32)
    loads[1].wait()
    key = jnp.dot(normed, wk[...], preferred_element_type=F32).astype(BF16).astype(F32)
    loads[2].wait()
    value = jnp.dot(normed, wv[...], preferred_element_type=F32).astype(BF16).astype(F32)

    for h in range(heads):
        q = query[:, h * DK : (h + 1) * DK]
        k = key[:, h * DK : (h + 1) * DK]
        v = value[:, h * DV : (h + 1) * DV]
        q = q * cosine + pltpu.roll(q, DK // 2, 1) * sine
        k = (k * cosine + pltpu.roll(k, DK // 2, 1) * sine) * np.float32(DK**-0.5)
        within = jnp.sum(q * k, axis=-1, keepdims=True) * v
        turned = q.T
        for b in range(n_rows):
            if h == 0 and b % per == 0:
                loads[3 + b // per].wait()
            carried[b : b + 1, :] = jnp.sum(
                turned[:, b : b + 1] * state[b, h], axis=0, keepdims=True
            )
        head = jnp.broadcast_to(t * heads + h, (1, 1)).astype(F32)
        decay = 1.0 - jnp.exp2(-2.0 - 2.0 * head)
        retained = decay * carried[...] + within
        centred = retained - jnp.mean(retained, axis=-1, keepdims=True)
        variance = jnp.mean(centred * centred, axis=-1, keepdims=True)
        normal = (
            centred * lax.rsqrt(variance + EPS) * head_gain[:, h * DV : (h + 1) * DV]
        ).astype(BF16)
        if h == 0:
            loads[3 + n_state].wait()
        product = jnp.dot(normal, wo[h * DV : (h + 1) * DV, :], preferred_element_type=F32)
        attended = product if h == 0 else attended + product
    attended = attended.astype(BF16)
    part[...] = attended

    pl.semaphore_wait(barrier, greetings(n_ep, n_x))

    sends = []
    for d in range(1, n_tp):
        copy = pltpu.make_async_remote_copy(
            src_ref=part,
            dst_ref=part_in.at[d - 1],
            send_sem=tp_send.at[d - 1],
            recv_sem=tp_recv.at[d - 1],
            device_id=to(e, (t + d) % n_tp),
            device_id_type=pl.DeviceIdType.MESH,
        )
        copy.start()
        sends.append(copy)
    total = attended.astype(F32)
    for copy in sends:
        copy.wait_recv()
    for d in range(1, n_tp):
        total = total + part_in[d - 1].astype(F32)
    resid_f = (token_f + total).astype(BF16).astype(F32)
    resid[...] = resid_f
    scale = lax.rsqrt(jnp.mean(resid_f * resid_f, axis=-1, keepdims=True) + EPS)
    mid = (resid_f * scale * norm_mid[...]).astype(BF16)
    for j in range(CORES):
        rows[e, j] = mid[:, j * half : (j + 1) * half]

    def row_copy(d):
        return pltpu.make_async_remote_copy(
            src_ref=rows.at[e, c],
            dst_ref=rows.at[e, c],
            send_sem=row_send.at[d],
            recv_sem=row_recv.at[d],
            device_id=to((e + d) % n_ep, t),
            device_id_type=pl.DeviceIdType.MESH,
        )

    def row_arrival(d):
        origin = (e + n_ep - d) % n_ep
        return pltpu.make_async_remote_copy(
            src_ref=rows.at[origin, c],
            dst_ref=rows.at[origin, c],
            send_sem=row_send.at[d],
            recv_sem=row_recv.at[d],
            device_id=to((e + d) % n_ep, t),
            device_id_type=pl.DeviceIdType.MESH,
        )

    def forward(d, lane):
        origin = (e + n_ep - d) % n_ep
        return pltpu.make_async_remote_copy(
            src_ref=rows.at[origin, lane],
            dst_ref=rows.at[origin, lane],
            send_sem=fwd_send.at[d],
            recv_sem=fwd_recv.at[d],
            device_id=to(e, sibling),
            device_id_type=pl.DeviceIdType.MESH,
        )

    each(1, n_ep, lambda d: row_copy(d).start())

    def relay(d):
        row_arrival(d).wait_recv()
        forward(d, c).start()

    each(1, n_ep, relay)
    each(1, n_ep, lambda d: forward(d, 1 - c).wait_recv())
    for copy in loads[4 + n_state :]:
        copy.wait()

    group = 8 if n_ep % 8 == 0 else n_ep
    span = group * n_rows

    def expert(i):
        block = rows[pl.ds(i * group, group)]
        gate_sum = jnp.zeros((span, gate.shape[0]), F32)
        up_sum = jnp.zeros((span, gate.shape[0]), F32)
        for j in range(CORES):
            piece = block[:, j].reshape(span, half)
            gate_sum += dot_rows(piece, gate[:, j * half : (j + 1) * half])
            up_sum += dot_rows(piece, up[:, j * half : (j + 1) * half])
        hidden[pl.ds(i * span, span), :] = (jax.nn.silu(gate_sum) * up_sum).astype(BF16)

    each(0, n_ep // group, expert)

    def columns(i, j, core):
        start = pl.multiple_of((j * CORES + core) * quarter, quarter)
        return jnp.dot(
            hidden[pl.ds(i * span, span), :],
            down[:, pl.ds(start, quarter)],
            preferred_element_type=F32,
        )

    pair_copies = []
    for j in range(n_x):

        def other(i, j=j):
            pair_out[j, pl.ds(i * group, group)] = (
                columns(i, j, 1 - c).astype(BF16).reshape(group, n_rows, quarter)
            )

        each(0, n_ep // group, other)
        copy = pltpu.make_async_remote_copy(
            src_ref=pair_out.at[j],
            dst_ref=pair_in.at[j],
            send_sem=pair_send.at[j],
            recv_sem=pair_recv.at[j],
            device_id=to(e, sibling),
            device_id_type=pl.DeviceIdType.MESH,
        )
        copy.start()
        pair_copies.append(copy)

    def return_copy(d, dx):
        target = (e + d) % n_ep
        lane = (x + dx) % n_x
        return pltpu.make_async_remote_copy(
            src_ref=share.at[lane, target],
            dst_ref=arrived.at[dx, d],
            send_sem=ret_send.at[dx, d],
            recv_sem=ret_recv.at[dx, d],
            device_id=to(target, lane * CORES + c),
            device_id_type=pl.DeviceIdType.MESH,
        )

    for dx in range(n_x):

        def own(i, dx=dx):
            mine = columns(i, (x + dx) % n_x, c)
            own_sum[dx, pl.ds(i * group, group)] = mine.reshape(group, n_rows, quarter)

        each(0, n_ep // group, own)
    for copy in pair_copies:
        copy.wait_recv()
    for dx in [*range(1, n_x), 0]:
        lane = (x + dx) % n_x

        def add(i, dx=dx, lane=lane):
            here = pl.ds(i * group, group)
            share[lane, here] = (own_sum[dx, here] + pair_in[lane, here].astype(F32)).astype(BF16)

        each(0, n_ep // group, add)
        each(0 if dx else 1, n_ep, lambda d, dx=dx: return_copy(d, dx).start())

    def mixing(d):
        expert_index = ((e + n_ep - d) % n_ep) // SPREAD
        wanted = jnp.broadcast_to(expert_index, (1, 1)).astype(F32)
        total = jnp.where(chosen[0] == wanted, weights[0], 0.0)
        for j in range(1, top_k):
            total = total + jnp.where(chosen[j] == wanted, weights[j], 0.0)
        return total

    start = pl.multiple_of(t * quarter, quarter)
    out_sum = resid[:, pl.ds(start, quarter)] + mixing(0) * share[x, e].astype(F32)
    if n_ep <= 8:
        for dx in [0, *range(1, n_x)]:
            for d in range(0 if dx else 1, n_ep):
                return_copy(d, dx).wait_recv()
                out_sum = out_sum + mixing(d) * arrived[dx, d].astype(F32)
    else:
        for dx in range(n_x):

            def gather(d, carry, dx=dx):
                return_copy(d, dx).wait_recv()
                return carry + mixing(d) * arrived[dx, d].astype(F32)

            out_sum = lax.fori_loop(0 if dx else 1, n_ep, gather, out_sum)
    out[...] = out_sum.astype(BF16)

    for copy in sends + pair_copies:
        copy.wait_send()

    def finish(d):
        row_copy(d).wait_send()
        forward(d, c).wait_send()
        return_copy(d, 0).wait_send()

    each(1, n_ep, finish)
    for dx in range(1, n_x):
        each(0, n_ep, lambda d, dx=dx: return_copy(d, dx).wait_send())


def greetings(n_ep, n_x):
    return n_x * (n_ep - 1) + (n_x - 1) + n_x


def body(
    n_ep,
    n_tp,
    tokens,
    seq_length,
    ret_state,
    norm_in,
    w_query,
    w_key,
    w_value,
    head_gain,
    w_output,
    norm_mid,
    route_expert,
    route_score,
    expert_gate,
    expert_up,
    expert_down,
):
    n_rows, width = tokens.shape
    quarter = width // n_tp
    half = width // CORES
    n_x = n_tp // CORES
    hidden_units = expert_gate.shape[2]
    angle = np.arange(DK, dtype=np.float64) % (DK // 2)
    inverse = jnp.asarray((10000.0 ** (-angle / (DK // 2))).astype(np.float32)[None, :])
    vmem = pl.BlockSpec(memory_space=pltpu.VMEM)
    anywhere = pl.BlockSpec(memory_space=pl.ANY)
    dma = pltpu.SemaphoreType.DMA
    return pl.pallas_call(
        functools.partial(kernel, n_ep, n_tp),
        out_shape=jax.ShapeDtypeStruct((n_rows, quarter), BF16),
        in_specs=[vmem] * 8 + [anywhere] * 8,
        out_specs=vmem,
        scratch_shapes=[
            pltpu.VMEM(ret_state.shape, F32),
            pltpu.VMEM(w_query.shape, BF16),
            pltpu.VMEM(w_key.shape, BF16),
            pltpu.VMEM(w_value.shape, BF16),
            pltpu.VMEM(w_output.shape, BF16),
            pltpu.VMEM((hidden_units, width), BF16),
            pltpu.VMEM((hidden_units, width), BF16),
            pltpu.VMEM(expert_down.shape[1:], BF16),
            pltpu.VMEM((n_rows, DV), F32),
            pltpu.VMEM((n_rows, width), BF16),
            pltpu.VMEM((n_tp - 1, n_rows, width), BF16),
            pltpu.VMEM((n_rows, width), F32),
            pltpu.VMEM((n_ep, CORES, n_rows, half), BF16),
            pltpu.VMEM((n_ep * n_rows, hidden_units), BF16),
            pltpu.VMEM((n_x, n_ep, n_rows, quarter), BF16),
            pltpu.VMEM((n_x, n_ep, n_rows, quarter), BF16),
            pltpu.VMEM((n_x, n_ep, n_rows, quarter), F32),
            pltpu.VMEM((n_x, n_ep, n_rows, quarter), BF16),
            pltpu.VMEM((n_x, n_ep, n_rows, quarter), BF16),
            dma((12,)),
            dma((n_tp - 1,)),
            dma((n_tp - 1,)),
            dma((n_ep,)),
            dma((n_ep,)),
            dma((n_ep,)),
            dma((n_ep,)),
            dma((n_x,)),
            dma((n_x,)),
            dma((n_x, n_ep)),
            dma((n_x, n_ep)),
        ],
        compiler_params=pltpu.CompilerParams(collective_id=0, has_side_effects=True),
    )(
        tokens,
        seq_length.reshape(1, n_rows),
        inverse,
        norm_in.reshape(1, width),
        head_gain.reshape(1, -1),
        norm_mid.reshape(1, width),
        route_expert.T,
        route_score.T,
        ret_state,
        w_query,
        w_key,
        w_value,
        w_output,
        jnp.swapaxes(expert_gate, 1, 2),
        jnp.swapaxes(expert_up, 1, 2),
        expert_down,
    )


def solution(mesh):
    placed = (
        P("ep", None),
        P("ep"),
        P("ep", "tp", None, None),
        P(),
        P(None, "tp"),
        P(None, "tp"),
        P(None, "tp"),
        P("tp"),
        P("tp", None),
        P(),
        P("ep", None),
        P("ep", None),
        P("ep", None, "tp"),
        P("ep", None, "tp"),
        P("ep", "tp", None),
    )
    step = functools.partial(body, mesh.shape["ep"], mesh.shape["tp"])
    return jax.shard_map(step, mesh=mesh, in_specs=placed, out_specs=P("ep", "tp"), check_vma=False)
```

time: 89.9 us -> 26.8 us (0.30)
  blocking collectives: 43.4 us -> 0 us
  Pallas kernels: 0 us -> 25.2 us
  waiting for transfers between devices: 16.5 us -> 0 us
  between operations: 13.6 us -> 0.01 us
  matrix products: 8.21 us -> 0 us
  other arithmetic: 4.82 us -> 0 us
  local copies, waits for them, and re-layouts: 2.74 us -> 1.3 us
    pallas_call x0 -> x1, Pallas kernels: none -> 25.2 us  [body(): pl.pallas_call(functools.partial(kernel, n_ep, n_tp), out_shape=jax.Shape...]
    all_to_all x2 -> x0, blocking collectives: 24.8 us -> none  [the longest x1 12.5 us: body(): lax.all_to_all(send_buffer, 'ep', split_axis=0, concat_axis=0, tiled=True)]
    reduce_scatter x1 -> x0, waiting for transfers between devices: 16.5 us -> none  [body(): lax.psum_scatter(down_part.astype(jnp.bfloat16), 'tp', scatter_dimension=...]
    psum x1 -> x0, blocking collectives: 12.9 us -> none  [body(): lax.psum(partial_value.astype(jnp.bfloat16), 'tp').astype(jnp.float32)]
    dot_general x9 -> x0, matrix products: 8.21 us -> none  [the longest x1 2.82 us: body(): down_part = jnp.dot(hidden, down_rows, preferred_element_type=jnp.float32)]
    all_gather x1 -> x0, blocking collectives: 5.76 us -> none  [body(): piece_cols = lax.all_gather(received, 'tp', axis=2, tiled=True)]
    reduce_sum x8 -> x0, other arithmetic: 2.34 us -> none  [the longest x1 0.88 us: body(): jnp.mean(token_f * token_f, axis=-1, keepdims=True) + EPS]
    reshape x4 -> x0, local copies, waits for them, and re-layouts: 0.9 us -> none  [the longest x1 0.81 us: body(): share.astype(jnp.bfloat16).reshape(groups, row_count, share.shape[1])]
  transfers between devices with their start and end apart: 1 -> 0, of which waited for: 1 -> 0; matrix products, arithmetic and copies ran while one was open for 0% -> 0% of each run, Pallas kernels for 0% -> 0%
where the time goes in v1:
time: 26.8 us; the launch traced here: 26.5 us
  Pallas kernels  25.2 us (94%)
  local copies, waits for them, and re-layouts  1.3 us (5%)
    pallas_call x1, Pallas kernels, body(): pl.pallas_call(functools.partial(kernel, n_ep, n_tp), out_shape=jax.Shape...  25.2 us
    unnamed x1, local copies, waits for them, and re-layouts  1.3 us

profile of v1, /device:TPU:0, one launch (start us, length us, event | category | flops | bytes accessed | tf_op | source)
XLA Modules:
  0.0 26.5 jit_solution(230747904740094889)
XLA Ops:
  0.0 25.2 %shard_map.154 = bf16[16,256]{1,0:T(8,128)(2,1)} custom-call(bf16[16,1024]{1,0:T(8,128)(2,1)} %tokens.1, s32[1,16]{1,0:T(1,128)} %bitcast.15, f32[1,128]{1,0:T(1,128)} %constant.2.clone.inverse, f32[1,1024]{1,0:T(1,128)} %bitcast.10, f32[1,256]{1,0:T(1,128)} %bitcast.12, f32[1,1024]{1,0:T(1,128)} %bitcast.11, s32[2,16]{1,0:T(2,128)} %bitcast.13, ...), custom_call_target="tpu_custom_call" | custom-call | tf_op jit(solution)/shard_map/pallas_call | solution.py:429
  25.2 1.3 %copy.18 = bf16[16,256]{1,0:T(8,128)(2,1)} copy(bf16[16,256]{1,0:T(8,128)(2,1)} %shard_map.154) | data formatting | bytes 16384

commit v2 on v1

--- a/solution.py
+++ b/solution.py
@@ -94,6 +94,8 @@
     own_sum,
     share,
     arrived,
+    round_sem,
+    ready_sem,
     load_sem,
     tp_send,
     tp_recv,
@@ -125,13 +127,17 @@
 
     barrier = pltpu.get_barrier_semaphore()
 
-    def greet(d):
-        for dx in range(n_x):
-            peer = to((e + d) % n_ep, ((x + dx) % n_x) * CORES + c)
-            pl.semaphore_signal(
-                barrier, inc=1, device_id=peer, device_id_type=pl.DeviceIdType.MESH
-            )
-
+    def signal(semaphore, peer):
+        pl.semaphore_signal(
+            semaphore, inc=1, device_id=peer, device_id_type=pl.DeviceIdType.MESH
+        )
+
+    powers = [1 << i for i in range(n_ep.bit_length() - 1)]
+    cube = [to(e + w * (1 - 2 * ((e // w) % 2)), t) for w in powers]
+    for d in range(1, n_tp):
+        signal(barrier, to(e, (t + d) % n_tp))
+    for peer in cube:
+        signal(barrier, peer)
     loads = []
     pairs = [(wq_hbm, wq), (wk_hbm, wk), (wv_hbm, wv)]
     for i in range(n_state):
@@ -146,14 +152,6 @@
         load = pltpu.make_async_copy(source, target, load_sem.at[i])
         load.start()
         loads.append(load)
-    for dx in range(1, n_x):
-        peer = to(e, ((x + dx) % n_x) * CORES + c)
-        pl.semaphore_signal(barrier, inc=1, device_id=peer, device_id_type=pl.DeviceIdType.MESH)
-    for dx in range(n_x):
-        peer = to(e, ((x + dx) % n_x) * CORES + 1 - c)
-        pl.semaphore_signal(barrier, inc=1, device_id=peer, device_id_type=pl.DeviceIdType.MESH)
-    each(1, n_ep, greet)
-
     token_f = tokens[...].astype(F32)
     scale = lax.rsqrt(jnp.mean(token_f * token_f, axis=-1, keepdims=True) + EPS)
     normed = (token_f * scale * norm_in[...]).astype(BF16)
@@ -212,7 +210,7 @@
     attended = attended.astype(BF16)
     part[...] = attended
 
-    pl.semaphore_wait(barrier, greetings(n_ep, n_x))
+    pl.semaphore_wait(barrier, n_tp - 1 + len(cube))
 
     sends = []
     for d in range(1, n_tp):
@@ -226,6 +224,13 @@
         )
         copy.start()
         sends.append(copy)
+
+    for i, peer in enumerate(cube[:-1]):
+        signal(round_sem.at[i], peer)
+        pl.semaphore_wait(round_sem.at[i], 1)
+    for dx in range(1, n_x):
+        signal(ready_sem, to(e, ((x + dx) % n_x) * CORES + c))
+
     total = attended.astype(F32)
     for copy in sends:
         copy.wait_recv()
@@ -345,6 +350,7 @@
         each(0, n_ep // group, own)
     for copy in pair_copies:
         copy.wait_recv()
+    pl.semaphore_wait(ready_sem, n_x - 1)
     for dx in [*range(1, n_x), 0]:
         lane = (x + dx) % n_x
 
@@ -391,10 +397,6 @@
     each(1, n_ep, finish)
     for dx in range(1, n_x):
         each(0, n_ep, lambda d, dx=dx: return_copy(d, dx).wait_send())
-
-
-def greetings(n_ep, n_x):
-    return n_x * (n_ep - 1) + (n_x - 1) + n_x
 
 
 def body(
@@ -451,6 +453,8 @@
             pltpu.VMEM((n_x, n_ep, n_rows, quarter), F32),
             pltpu.VMEM((n_x, n_ep, n_rows, quarter), BF16),
             pltpu.VMEM((n_x, n_ep, n_rows, quarter), BF16),
+            pltpu.SemaphoreType.REGULAR((n_ep.bit_length(),)),
+            pltpu.SemaphoreType.REGULAR,
             dma((12,)),
             dma((n_tp - 1,)),
             dma((n_tp - 1,)),

time: 26.8 us -> 25.6 us (0.955)
  Pallas kernels: 25.2 us -> 24.1 us
    pallas_call x1, Pallas kernels: 25.2 us -> 24.1 us  [body(): pl.pallas_call(functools.partial(kernel, n_ep, n_tp), out_shape=jax.Shape...]
where the time goes in v2:
time: 25.6 us; the launch traced here: 25.4 us
  Pallas kernels  24.1 us (94%)
  local copies, waits for them, and re-layouts  1.3 us (5%)
    pallas_call x1, Pallas kernels, body(): pl.pallas_call(functools.partial(kernel, n_ep, n_tp), out_shape=jax.Shape...  24.1 us
    unnamed x1, local copies, waits for them, and re-layouts  1.3 us

profile of v2, /device:TPU:0, one launch (start us, length us, event | category | flops | bytes accessed | tf_op | source)
XLA Modules:
  0.0 25.4 jit_solution(4106622721775963309)
XLA Ops:
  0.0 24.1 %shard_map.154 = bf16[16,256]{1,0:T(8,128)(2,1)} custom-call(bf16[16,1024]{1,0:T(8,128)(2,1)} %tokens.1, s32[1,16]{1,0:T(1,128)} %bitcast.15, f32[1,128]{1,0:T(1,128)} %constant.2.clone.inverse, f32[1,1024]{1,0:T(1,128)} %bitcast.10, f32[1,256]{1,0:T(1,128)} %bitcast.12, f32[1,1024]{1,0:T(1,128)} %bitcast.11, s32[2,16]{1,0:T(2,128)} %bitcast.13, ...), custom_call_target="tpu_custom_call" | custom-call | tf_op jit(solution)/shard_map/pallas_call | solution.py:431
  24.1 1.3 %copy.18 = bf16[16,256]{1,0:T(8,128)(2,1)} copy(bf16[16,256]{1,0:T(8,128)(2,1)} %shard_map.154) | data formatting | bytes 16384
